TPU v7x, 32 devices: a whole 2x2x4 slice. The times are simulated.
32 devices in a mesh: sp: 16 (over z, y, x), tp: 2 (over core).
Axes of the slice: x: 2, y: 2, z: 4, core: 2. Of those that a mesh axis runs over, the one named last changes fastest.
Arguments:
- tokens: bfloat16 [2048, 1024], P('sp', 'tp'), may hold values from -6 to 6
- norm_gain: float32 [1024], P('tp'), may hold values from 0.1 to 1.9
- query_weight: bfloat16 [1024, 1024], P('sp', 'tp'), may hold values from -0.1875 to 0.1875
- key_weight: bfloat16 [1024, 512], P('sp', 'tp'), may hold values from -0.1875 to 0.1875
- value_weight: bfloat16 [1024, 512], P('sp', 'tp'), may hold values from -0.1875 to 0.1875
- conv_in_weight: bfloat16 [1024, 1024], P('sp', 'tp'), may hold values from -0.1875 to 0.1875
- pre_weight: bfloat16 [1024, 1024], P('sp', 'tp'), may hold values from -0.1875 to 0.1875
- post_weight: bfloat16 [1024, 1024], P('sp', 'tp'), may hold values from -0.1875 to 0.1875
- attn_gate_weight: bfloat16 [1024, 1024], P('sp', 'tp'), may hold values from -0.1875 to 0.1875
- conv_gate_weight: bfloat16 [1024, 1024], P('sp', 'tp'), may hold values from -0.1875 to 0.1875
- sink_logit: float32 [16], P('tp'), may hold values from 1 to 5
- conv_taps: float32 [3, 1024], P(None, 'tp'), may hold values from -3 to 3
- attn_out_weight: bfloat16 [1024, 1024], P('tp', 'sp'), may hold values from -1 to 1
- conv_out_weight: bfloat16 [1024, 1024], P('tp', 'sp'), may hold values from -0.1875 to 0.1875
Outputs:
- merged: bfloat16 [2048, 1024], P('sp', 'tp')
All inputs are finite; a program needn't handle non-finite values.
Results may differ from a plain program's by a relative error of at most 0.003.
Values may be sent and summed in bfloat16 or wider, within the bound.
A program may use at most 64 MiB of HBM per device.

v0:
```python
import jax
import jax.numpy as jnp
from jax import lax
from jax.sharding import PartitionSpec as P

HEAD_DIM = 64
WINDOW = 64
epsilon = 1e-06
negative = -1e30


def folded(shard, axis, dim, absorb, state):
    everything = jax.tree.map(lambda a: lax.all_gather(a, axis, axis=dim, tiled=True), shard)
    return absorb(state, everything, jnp.int32(0))


def for_sending(shard):

    def short(part):
        return part.astype(jnp.bfloat16) if part.dtype == jnp.float32 else part

    return jax.tree.map(short, shard)


def extended(shard, sides, width, wrap):
    for axis, dim in sides:
        devices, length = (lax.axis_size(axis), shard.shape[dim])
        up = [(i, (i + 1) % devices) for i in range(devices if wrap else devices - 1)]
        down = [(j, i) for i, j in up]
        last = lax.slice_in_dim(shard, length - width, length, axis=dim)
        first = lax.slice_in_dim(shard, 0, width, axis=dim)
        before = lax.ppermute(last, axis, up)
        after = lax.ppermute(first, axis, down)
        shard = jnp.concatenate([before, shard, after], axis=dim)
    return shard


def summed_rows(product, width, axis):
    whole = product(jnp.int32(0), width * lax.axis_size(axis))
    return lax.psum_scatter(whole, axis, scatter_dimension=0, tiled=True)


def window_mix(queries, key_rows, value_rows, sink_cols, first, seq_total):
    score_scale = queries.shape[-1] ** (-0.5)
    scores = (
        jnp.einsum("qhgd,khd->hgqk", queries, key_rows, preferred_element_type=jnp.float32)
        * score_scale
    )
    qpos = first + jnp.arange(queries.shape[0], dtype=jnp.int32)
    kpos = first - WINDOW + jnp.arange(key_rows.shape[0], dtype=jnp.int32)
    allowed = (
        (jnp.abs(qpos[:, None] - kpos[None, :]) <= WINDOW)
        & (kpos >= 0)[None, :]
        & (kpos < seq_total)[None, :]
    )
    scores = jnp.where(allowed, scores, negative)
    column = jnp.broadcast_to(sink_cols[:, :, None, None], scores.shape[:-1] + (1,))
    weights_soft = jax.nn.softmax(jnp.concatenate([scores, column], axis=-1), axis=-1)[..., :-1]
    return jnp.einsum(
        "hgqk,khd->qhgd",
        weights_soft,
        value_rows.astype(jnp.float32),
        precision=lax.Precision.HIGHEST,
    )


def short_conv(padded, conv_taps):
    return (
        conv_taps[0][None, :] * padded[:-2]
        + conv_taps[1][None, :] * padded[1:-1]
        + conv_taps[2][None, :] * padded[2:]
    )


def per_device(
    tokens,
    norm_gain,
    query_weight,
    key_weight,
    value_weight,
    conv_in_weight,
    pre_weight,
    post_weight,
    attn_gate_weight,
    conv_gate_weight,
    sink_logit,
    conv_taps,
    attn_out_weight,
    conv_out_weight,
):
    tok_rows = tokens.shape[0]
    widened = tokens.astype(jnp.float32)
    row_sums = lax.psum(jnp.sum(widened * widened, axis=1), "tp")
    features = tokens.shape[1] * lax.axis_size("tp")
    normed = (
        widened * lax.rsqrt(row_sums[:, None] / features + epsilon) * norm_gain[None, :]
    ).astype(jnp.bfloat16)
    collected = (
        lax.all_gather(query_weight, "sp", axis=0, tiled=True),
        lax.all_gather(key_weight, "sp", axis=0, tiled=True),
        lax.all_gather(value_weight, "sp", axis=0, tiled=True),
        lax.all_gather(conv_in_weight, "sp", axis=0, tiled=True),
        lax.all_gather(pre_weight, "sp", axis=0, tiled=True),
        lax.all_gather(post_weight, "sp", axis=0, tiled=True),
        lax.all_gather(attn_gate_weight, "sp", axis=0, tiled=True),
        lax.all_gather(conv_gate_weight, "sp", axis=0, tiled=True),
    )
    stacked = jnp.concatenate(collected, axis=1)

    def add_rows(carry_sum, segment, first):
        rows_here = lax.dynamic_slice_in_dim(stacked, first, segment.shape[1], 0)
        return carry_sum + jnp.dot(segment, rows_here, preferred_element_type=jnp.float32)

    projected = folded(
        normed, "tp", 1, add_rows, jnp.zeros((tok_rows, stacked.shape[1]), jnp.float32)
    )
    pieces = []
    offset = 0
    for weight in collected:
        pieces.append(projected[:, offset : offset + weight.shape[1]])
        offset = offset + weight.shape[1]
    queries, key_rows, value_rows, conv_in, pre_gate, post_gate = [
        part_rows.astype(jnp.bfloat16) for part_rows in pieces[:6]
    ]
    attn_gate = pieces[6]
    conv_gate = pieces[7]
    conv_mix = (pre_gate.astype(jnp.float32) * conv_in.astype(jnp.float32)).astype(jnp.bfloat16)
    kv_width = key_rows.shape[1]
    kv_pad = extended(
        for_sending(jnp.concatenate([key_rows, value_rows], axis=1)), (("sp", 0),), WINDOW, False
    )
    key_pad = kv_pad[:, :kv_width]
    value_pad = kv_pad[:, kv_width:]
    conv_pad = extended(conv_mix, (("sp", 0),), 1, False)
    kv_local = kv_width // HEAD_DIM
    group_size = queries.shape[1] // kv_width
    first_row = lax.axis_index("sp") * tok_rows
    attended = window_mix(
        queries.reshape(tok_rows, kv_local, group_size, HEAD_DIM),
        key_pad.reshape(-1, kv_local, HEAD_DIM),
        value_pad.reshape(-1, kv_local, HEAD_DIM),
        sink_logit.reshape(kv_local, group_size),
        first_row,
        tok_rows * lax.axis_size("sp"),
    )
    attended = attended.reshape(tok_rows, -1).astype(jnp.bfloat16)
    conv_out = (
        post_gate.astype(jnp.float32) * short_conv(conv_pad.astype(jnp.float32), conv_taps)
    ).astype(jnp.bfloat16)
    attn_full, conv_full = (
        lax.all_gather(attn_out_weight, "sp", axis=1, tiled=True),
        lax.all_gather(conv_out_weight, "sp", axis=1, tiled=True),
    )

    def attn_term(first, number):
        columns = lax.dynamic_slice_in_dim(attn_full, first, number, 1)
        return jnp.dot(attended, columns, preferred_element_type=jnp.float32).T

    def conv_term(first, number):
        columns = lax.dynamic_slice_in_dim(conv_full, first, number, 1)
        return jnp.dot(conv_out, columns, preferred_element_type=jnp.float32).T

    out_rows = attn_gate.shape[1]

    def both_terms(first, number):
        return jnp.concatenate([attn_term(first, number), conv_term(first, number)], axis=1)

    summed = summed_rows(both_terms, out_rows, "tp")
    branch_attn = summed[:, :tok_rows].T
    branch_conv = summed[:, tok_rows:].T
    return (
        jax.nn.sigmoid(attn_gate) * branch_attn + jax.nn.sigmoid(conv_gate) * branch_conv
    ).astype(jnp.bfloat16)


def solution(mesh):
    return jax.shard_map(
        per_device,
        mesh=mesh,
        in_specs=(
            P("sp", "tp"),
            P("tp"),
            P("sp", "tp"),
            P("sp", "tp"),
            P("sp", "tp"),
            P("sp", "tp"),
            P("sp", "tp"),
            P("sp", "tp"),
            P("sp", "tp"),
            P("sp", "tp"),
            P("tp"),
            P(None, "tp"),
            P("tp", "sp"),
            P("tp", "sp"),
        ),
        out_specs=P("sp", "tp"),
        check_vma=False,
    )
```

profile of v0, /device:TPU:0, one launch (start us, length us, event | category | flops | bytes accessed | tf_op | source)
XLA Modules:
  0.0 485.7 jit_solution(2736074384034451135)
XLA Ops:
  12.1 45.7 %all_gather.35 = bf16[1024,256]{1,0:T(8,128)(2,1)S(1)} all-gather(bf16[64,256]{1,0:T(8,128)(2,1)} %param.17), channel_id=1, replica_groups=mesh['sp'=16,'tp'=2] {'sp'}, dimensions={0}, use_global_device_ids=true | all-gather | bytes 557056 | tf_op jit(solution)/shard_map/all_gather | solution.py:100
  57.8 40.3 %all_gather.36 = bf16[1024,256]{1,0:T(8,128)(2,1)S(1)} all-gather(bf16[64,256]{1,0:T(8,128)(2,1)} %param.18), channel_id=1, replica_groups=mesh['sp'=16,'tp'=2] {'sp'}, dimensions={0}, use_global_device_ids=true | all-gather | bytes 557056 | tf_op jit(solution)/shard_map/all_gather | solution.py:101
  98.1 1.0 fusion.4
  99.1 2.5 psum.7
  101.6 1.0 fusion.6
  102.6 2.0 all_gather.33
  104.6 1.3 broadcast_in_dim.27
  105.9 1.4 fusion.35
  108.1 2.3 constant_dynamic-update-slice_fusion.7
  112.2 15.1 %all-gather.11.cloned.1.call-done = bf16[1024,512]{1,0:T(8,128)(2,1)} async-done(((bf16[64,512]{1,0:T(8,128)(2,1)}), bf16[1024,512]{1,0:T(8,128)(2,1)}) %all-gather.11.cloned.1.call-update) | async-done | bytes 1048592 | tf_op jit(solution)/shard_map/all_gather | solution.py:102
  127.3 2.3 constant_dynamic-update-slice_fusion.4
  129.6 54.4 %all-gather.13.cloned.1.call-done = bf16[1024,512]{1,0:T(8,128)(2,1)} async-done(((bf16[64,512]{1,0:T(8,128)(2,1)}), bf16[1024,512]{1,0:T(8,128)(2,1)}) %all-gather.13.cloned.1.call-update) | async-done | bytes 1048592 | tf_op jit(solution)/shard_map/all_gather | solution.py:103
  184.0 2.3 constant_dynamic-update-slice_fusion.3
  186.3 54.3 %all-gather.15.cloned.1.call-done = bf16[1024,512]{1,0:T(8,128)(2,1)} async-done(((bf16[64,512]{1,0:T(8,128)(2,1)}), bf16[1024,512]{1,0:T(8,128)(2,1)}) %all-gather.15.cloned.1.call-update) | async-done | bytes 1048592 | tf_op jit(solution)/shard_map/all_gather | solution.py:104
  240.6 2.3 constant_dynamic-update-slice_fusion.2
  242.9 54.2 %all-gather.17.cloned.1.call-done = bf16[1024,512]{1,0:T(8,128)(2,1)} async-done(((bf16[64,512]{1,0:T(8,128)(2,1)}), bf16[1024,512]{1,0:T(8,128)(2,1)}) %all-gather.17.cloned.1.call-update) | async-done | bytes 1048592 | tf_op jit(solution)/shard_map/all_gather | solution.py:105
  297.1 2.3 constant_dynamic-update-slice_fusion.1
  299.5 54.2 %all-gather.19.cloned.1.call-done = bf16[1024,512]{1,0:T(8,128)(2,1)} async-done(((bf16[64,512]{1,0:T(8,128)(2,1)}), bf16[1024,512]{1,0:T(8,128)(2,1)}) %all-gather.19.cloned.1.call-update) | async-done | bytes 1048592 | tf_op jit(solution)/shard_map/all_gather | solution.py:106
  353.7 2.3 constant_dynamic-update-slice_fusion
  356.0 4.2 fusion.36
  361.0 3.3 collective-permute-start.2
  364.3 1.3 collective-permute-start.3
  366.3 5.2 %collective-permute-start = (bf16[64,512]{1,0:T(8,128)(2,1)}, bf16[64,512]{1,0:T(8,128)(2,1)}, u32[]{:S(2)}, u32[]{:S(2)}) collective-permute-start(bf16[64,512]{1,0:T(8,128)(2,1)} %get-tuple-element.9), channel_id=1, source_target_pairs={{0,2},{2,4},{4,6},{6,8},{8,10},{10,12},{12,14},{14,16},{16,18},{18... | collective-permute-start | bytes 196616 | tf_op jit(solution)/shard_map/ppermute | solution.py:32
  371.5 1.3 collective-permute-start.1
  373.5 36.9 %all-gather.23.cloned.1.call-done = bf16[512,1024]{0,1:T(8,128)(2,1)} async-done(((bf16[512,64]{0,1:T(8,128)(2,1)}), bf16[512,1024]{0,1:T(8,128)(2,1)}) %all-gather.23.cloned.1.call-update) | async-done | bytes 1048592 | tf_op jit(solution)/shard_map/all_gather | solution.py:152
  410.5 1.7 convolution_bitcast_fusion
  413.4 1.3 fusion.37
  416.9 50.3 %all-gather.21.cloned.1.call-done = bf16[512,1024]{0,1:T(8,128)(2,1)} async-done(((bf16[512,64]{0,1:T(8,128)(2,1)}), bf16[512,1024]{0,1:T(8,128)(2,1)}) %all-gather.21.cloned.1.call-update) | async-done | bytes 1048592 | tf_op jit(solution)/shard_map/all_gather | solution.py:151
  467.2 1.7 convolution_bitcast_fusion.1
  468.9 1.1 pad_maximum_fusion
  470.0 7.4 %reduce-scatter.2.cloned.1.call-done = f32[512,256]{0,1:T(8,128)} async-done(((f32[1024,256]{0,1:T(8,128)}), f32[512,256]{0,1:T(8,128)}) %reduce-scatter.2.cloned.1.call-update) | async-done | bytes 524304 | tf_op jit(solution)/shard_map/reduce_scatter | solution.py:40
  477.3 1.8 fusion.9
  (44 shorter events, 13.6 us)
Async XLA Ops:
  6.5 101.6 %all-gather.9.cloned.1.call-start = ((), (), s32[]{:S(2)}) async-start(), calls=%async_computation.1 | async-start | bytes 1114112 | tf_op jit(solution)/shard_map/all_gather | solution.py:99
  7.3 120.0 %all-gather.11.cloned.1.call-start = ((), (), s32[]{:S(2)}) async-start(), calls=%async_computation.2 | async-start | bytes 1114112 | tf_op jit(solution)/shard_map/all_gather | solution.py:102
  8.0 176.0 %all-gather.13.cloned.1.call-start = ((), (), s32[]{:S(2)}) async-start(), calls=%async_computation.3 | async-start | bytes 1114112 | tf_op jit(solution)/shard_map/all_gather | solution.py:103
  8.7 231.8 %all-gather.15.cloned.1.call-start = ((), (), s32[]{:S(2)}) async-start(), calls=%async_computation.4 | async-start | bytes 1114112 | tf_op jit(solution)/shard_map/all_gather | solution.py:104
  9.3 287.8 %all-gather.17.cloned.1.call-start = ((), (), s32[]{:S(2)}) async-start(), calls=%async_computation.5 | async-start | bytes 1114112 | tf_op jit(solution)/shard_map/all_gather | solution.py:105
  9.9 343.8 %all-gather.19.cloned.1.call-start = ((), (), s32[]{:S(2)}) async-start(), calls=%async_computation.6 | async-start | bytes 1114112 | tf_op jit(solution)/shard_map/all_gather | solution.py:106
  10.5 400.0 %all-gather.23.cloned.1.call-start = ((), (), s32[]{:S(2)}) async-start(), calls=%async_computation.8 | async-start | bytes 1114112 | tf_op jit(solution)/shard_map/all_gather | solution.py:152
  11.2 455.9 %all-gather.21.cloned.1.call-start = ((), (), s32[]{:S(2)}) async-start(), calls=%async_computation.7 | async-start | bytes 1114112 | tf_op jit(solution)/shard_map/all_gather | solution.py:151
  12.0 465.4 %reduce-scatter.2.cloned.1.call-start = ((), (), s32[]{:S(2)}) async-start(), calls=%async_computation.9 | async-start | bytes 1572864 | tf_op jit(solution)/shard_map/reduce_scatter | solution.py:40
  361.0 12.5 %collective-permute-start.2 = (bf16[1,512]{1,0:T(2,128)(2,1)S(1)}, bf16[1,512]{1,0:T(2,128)(2,1)S(1)}, u32[]{:S(2)}, u32[]{:S(2)}) collective-permute-start(bf16[1,512]{1,0:T(2,128)(2,1)S(1)} %get-tuple-element.13), channel_id=1, source_target_pairs={{0,2},{2,4},{4,6},{6,8},{8,10},{10,12},{12,14},{14,16},{16,18},{18... | collective-permute-start | bytes 3080 | tf_op jit(solution)/shard_map/ppermute | solution.py:32
  364.3 9.2 %collective-permute-start.3 = (bf16[1,512]{1,0:T(2,128)(2,1)S(1)}, bf16[1,512]{1,0:T(2,128)(2,1)S(1)}, u32[]{:S(2)}, u32[]{:S(2)}) collective-permute-start(bf16[1,512]{1,0:T(2,128)(2,1)S(1)} %get-tuple-element.14), channel_id=1, source_target_pairs={{2,0},{4,2},{6,4},{8,6},{10,8},{12,10},{14,12},{16,14},{18,16},{20... | collective-permute-start | bytes 3080 | tf_op jit(solution)/shard_map/ppermute | solution.py:33
  366.3 45.9 %collective-permute-start = (bf16[64,512]{1,0:T(8,128)(2,1)}, bf16[64,512]{1,0:T(8,128)(2,1)}, u32[]{:S(2)}, u32[]{:S(2)}) collective-permute-start(bf16[64,512]{1,0:T(8,128)(2,1)} %get-tuple-element.9), channel_id=1, source_target_pairs={{0,2},{2,4},{4,6},{6,8},{8,10},{10,12},{12,14},{14,16},{16,18},{18... | collective-permute-start | bytes 196616 | tf_op jit(solution)/shard_map/ppermute | solution.py:32
  371.5 40.7 %collective-permute-start.1 = (bf16[64,512]{1,0:T(8,128)(2,1)}, bf16[64,512]{1,0:T(8,128)(2,1)}, u32[]{:S(2)}, u32[]{:S(2)}) collective-permute-start(bf16[64,512]{1,0:T(8,128)(2,1)} %get-tuple-element.10), channel_id=1, source_target_pairs={{2,0},{4,2},{6,4},{8,6},{10,8},{12,10},{14,12},{16,14},{18,16},{20... | collective-permute-start | bytes 196616 | tf_op jit(solution)/shard_map/ppermute | solution.py:33
Sparse Core Ops, SparseCore 0:
  10.1 59.5 all-gather.8
  72.5 54.7 all-gather.10
  130.1 53.9 all-gather.12
  186.6 53.9 all-gather.14
  243.2 53.9 all-gather.16
  299.8 53.9 all-gather.18
  356.5 53.9 all-gather.22
  413.2 53.9 all-gather.20
  470.1 7.2 reduce-scatter.1
where the time goes:
time: 486 us
  waiting for transfers between devices  332 us (68%)
  blocking collectives  90.5 us (19%)
  local copies, waits for them, and re-layouts  21.5 us (4%)
  between operations  13.4 us (3%)
  starting transfers between devices  11.4 us (2%)
  matrix products  9.44 us (2%)
  other arithmetic  7.67 us (2%)
    all_gather x1, waiting for transfers between devices, per_device(): lax.all_gather(pre_weight, 'sp', axis=0, tiled=True)  54.4 us
    all_gather x1, waiting for transfers between devices, per_device(): lax.all_gather(post_weight, 'sp', axis=0, tiled=True)  54.3 us
    all_gather x1, waiting for transfers between devices, per_device(): lax.all_gather(attn_gate_weight, 'sp', axis=0, tiled=True)  54.2 us
    all_gather x1, waiting for transfers between devices, per_device(): lax.all_gather(conv_gate_weight, 'sp', axis=0, tiled=True)  54.2 us
    all_gather x1, waiting for transfers between devices, per_device(): lax.all_gather(attn_out_weight, 'sp', axis=1, tiled=True)  50.3 us
    all_gather x1, blocking collectives, per_device(): lax.all_gather(key_weight, 'sp', axis=0, tiled=True)  45.7 us
    all_gather x1, blocking collectives, per_device(): lax.all_gather(value_weight, 'sp', axis=0, tiled=True)  40.3 us
    all_gather x1, waiting for transfers between devices, per_device(): lax.all_gather(conv_out_weight, 'sp', axis=1, tiled=True)  36.9 us
  transfers between devices with their start and end apart: 13, of which 8 were waited for; matrix products, arithmetic and copies ran while one was open for 7% of the time, Pallas kernels for 0%

commit v1 on v0

--- a/solution.py
+++ b/solution.py
@@ -103,7 +103,9 @@
         lax.all_gather(pre_weight, "sp", axis=0, tiled=True),
         lax.all_gather(post_weight, "sp", axis=0, tiled=True),
         lax.all_gather(attn_gate_weight, "sp", axis=0, tiled=True),
-        lax.all_gather(conv_gate_weight, "sp", axis=0, tiled=True),
+        jnp.concatenate(
+            lax.all_to_all(jnp.stack([conv_gate_weight] * lax.axis_size("sp")), "sp", 0, 0), axis=0
+        ),
     )
     stacked = jnp.concatenate(collected, axis=1)
 

time: 486 us -> 436 us (0.90)
  waiting for transfers between devices: 332 us -> 272 us
  starting transfers between devices: 11.4 us -> 19.7 us
    all_gather x1 -> x0, waiting for transfers between devices: 54.2 us -> none  [per_device(): lax.all_gather(conv_gate_weight, 'sp', axis=0, tiled=True)]
    all_to_all x0 -> x1, starting transfers between devices: none -> 8.34 us  [per_device(): lax.all_to_all(jnp.stack([conv_gate_weight] * lax.axis_size('sp')), 'sp',...]
  transfers between devices with their start and end apart: 13 -> 13, of which waited for: 8 -> 7; matrix products, arithmetic and copies ran while one was open for 7% -> 8% of each run, Pallas kernels for 0% -> 0%
where the time goes in v1:
time: 436 us; the launch traced here: 435 us
  waiting for transfers between devices  272 us (62%)
  blocking collectives  90.8 us (21%)
  local copies, waits for them, and re-layouts  22.1 us (5%)
  starting transfers between devices  19.7 us (5%)
  between operations  13.7 us (3%)
  matrix products  9.45 us (2%)
  other arithmetic  7.61 us (2%)
    all_gather x1, waiting for transfers between devices, per_device(): lax.all_gather(pre_weight, 'sp', axis=0, tiled=True)  54.4 us
    all_gather x1, waiting for transfers between devices, per_device(): lax.all_gather(attn_gate_weight, 'sp', axis=0, tiled=True)  54.3 us
    all_gather x1, waiting for transfers between devices, per_device(): lax.all_gather(post_weight, 'sp', axis=0, tiled=True)  54.2 us
    all_gather x1, waiting for transfers between devices, per_device(): lax.all_gather(attn_out_weight, 'sp', axis=1, tiled=True)  50.4 us
    all_gather x1, blocking collectives, per_device(): lax.all_gather(key_weight, 'sp', axis=0, tiled=True)  46.1 us
    all_gather x1, blocking collectives, per_device(): lax.all_gather(value_weight, 'sp', axis=0, tiled=True)  40.3 us
    all_gather x1, waiting for transfers between devices, per_device(): lax.all_gather(conv_out_weight, 'sp', axis=1, tiled=True)  35.7 us
    unnamed x7, local copies, waits for them, and re-layouts  13.4 us
  transfers between devices with their start and end apart: 13, of which 7 were waited for; matrix products, arithmetic and copies ran while one was open for 8% of the time, Pallas kernels for 0%

profile of v1, /device:TPU:0, one launch (start us, length us, event | category | flops | bytes accessed | tf_op | source)
XLA Modules:
  0.0 435.3 jit_solution(15340231496960105664)
XLA Ops:
  10.5 1.9 stack.2
  12.4 8.3 %all-to-all-start = ((bf16[16,64,512]{2,1,0:T(8,128)(2,1)}), bf16[16,64,512]{2,1,0:T(8,128)(2,1)S(1)}, u32[]{:S(2)}, u32[]{:S(2)}) async-start(bf16[16,64,512]{2,1,0:T(8,128)(2,1)} %stack.2), calls=%async_computation | async-start | bytes 2097152 | tf_op jit(solution)/shard_map/all_to_all | solution.py:107
  21.6 1.0 fusion.4
  22.6 2.5 psum.7
  26.1 1.3 broadcast_in_dim.27
  27.4 2.0 all_gather.30
  29.4 1.4 fusion.35
  31.6 46.1 %all_gather.32 = bf16[1024,256]{1,0:T(8,128)(2,1)S(1)} all-gather(bf16[64,256]{1,0:T(8,128)(2,1)} %param.17), channel_id=1, replica_groups=mesh['sp'=16,'tp'=2] {'sp'}, dimensions={0}, use_global_device_ids=true | all-gather | bytes 557056 | tf_op jit(solution)/shard_map/all_gather | solution.py:100
  77.6 40.3 %all_gather.33 = bf16[1024,256]{1,0:T(8,128)(2,1)S(1)} all-gather(bf16[64,256]{1,0:T(8,128)(2,1)} %param.18), channel_id=1, replica_groups=mesh['sp'=16,'tp'=2] {'sp'}, dimensions={0}, use_global_device_ids=true | all-gather | bytes 557056 | tf_op jit(solution)/shard_map/all_gather | solution.py:101
  118.0 2.3 constant_dynamic-update-slice_fusion.7
  122.1 11.2 %all-gather.10.cloned.1.call-done = bf16[1024,512]{1,0:T(8,128)(2,1)} async-done(((bf16[64,512]{1,0:T(8,128)(2,1)}), bf16[1024,512]{1,0:T(8,128)(2,1)}) %all-gather.10.cloned.1.call-update) | async-done | bytes 1048592 | tf_op jit(solution)/shard_map/all_gather | solution.py:102
  133.3 2.3 constant_dynamic-update-slice_fusion.4
  135.6 54.4 %all-gather.12.cloned.1.call-done = bf16[1024,512]{1,0:T(8,128)(2,1)} async-done(((bf16[64,512]{1,0:T(8,128)(2,1)}), bf16[1024,512]{1,0:T(8,128)(2,1)}) %all-gather.12.cloned.1.call-update) | async-done | bytes 1048592 | tf_op jit(solution)/shard_map/all_gather | solution.py:103
  190.0 2.4 constant_dynamic-update-slice_fusion.3
  192.4 54.2 %all-gather.14.cloned.1.call-done = bf16[1024,512]{1,0:T(8,128)(2,1)} async-done(((bf16[64,512]{1,0:T(8,128)(2,1)}), bf16[1024,512]{1,0:T(8,128)(2,1)}) %all-gather.14.cloned.1.call-update) | async-done | bytes 1048592 | tf_op jit(solution)/shard_map/all_gather | solution.py:104
  246.6 2.3 constant_dynamic-update-slice_fusion.2
  248.9 54.3 %all-gather.16.cloned.1.call-done = bf16[1024,512]{1,0:T(8,128)(2,1)} async-done(((bf16[64,512]{1,0:T(8,128)(2,1)}), bf16[1024,512]{1,0:T(8,128)(2,1)}) %all-gather.16.cloned.1.call-update) | async-done | bytes 1048592 | tf_op jit(solution)/shard_map/all_gather | solution.py:105
  303.2 2.3 constant_dynamic-update-slice_fusion.1
  305.5 1.1 constant_dynamic-update-slice_fusion
  306.5 4.2 fusion.36
  311.5 3.3 collective-permute-start.2
  314.8 1.3 collective-permute-start.3
  316.8 5.2 %collective-permute-start = (bf16[64,512]{1,0:T(8,128)(2,1)}, bf16[64,512]{1,0:T(8,128)(2,1)}, u32[]{:S(2)}, u32[]{:S(2)}) collective-permute-start(bf16[64,512]{1,0:T(8,128)(2,1)} %get-tuple-element.9), channel_id=1, source_target_pairs={{0,2},{2,4},{4,6},{6,8},{8,10},{10,12},{12,14},{14,16},{16,18},{18... | collective-permute-start | bytes 196616 | tf_op jit(solution)/shard_map/ppermute | solution.py:32
  322.0 1.3 collective-permute-start.1
  324.1 35.7 %all-gather.20.cloned.1.call-done = bf16[512,1024]{0,1:T(8,128)(2,1)} async-done(((bf16[512,64]{0,1:T(8,128)(2,1)}), bf16[512,1024]{0,1:T(8,128)(2,1)}) %all-gather.20.cloned.1.call-update) | async-done | bytes 1048592 | tf_op jit(solution)/shard_map/all_gather | solution.py:154
  359.7 1.7 convolution_bitcast_fusion
  362.7 1.3 fusion.37
  366.1 50.4 %all-gather.18.cloned.1.call-done = bf16[512,1024]{0,1:T(8,128)(2,1)} async-done(((bf16[512,64]{0,1:T(8,128)(2,1)}), bf16[512,1024]{0,1:T(8,128)(2,1)}) %all-gather.18.cloned.1.call-update) | async-done | bytes 1048592 | tf_op jit(solution)/shard_map/all_gather | solution.py:153
  416.4 1.7 convolution_bitcast_fusion.1
  418.2 1.1 pad_maximum_fusion
  419.2 7.4 %reduce-scatter.2.cloned.1.call-done = f32[512,256]{0,1:T(8,128)} async-done(((f32[1024,256]{0,1:T(8,128)}), f32[512,256]{0,1:T(8,128)}) %reduce-scatter.2.cloned.1.call-update) | async-done | bytes 524304 | tf_op jit(solution)/shard_map/reduce_scatter | solution.py:40
  426.6 1.8 fusion.9
  (44 shorter events, 13.7 us)
Async XLA Ops:
  6.5 111.4 %all-gather.8.cloned.1.call-start = ((), (), s32[]{:S(2)}) async-start(), calls=%async_computation.2 | async-start | bytes 1114112 | tf_op jit(solution)/shard_map/all_gather | solution.py:99
  7.3 126.1 %all-gather.10.cloned.1.call-start = ((), (), s32[]{:S(2)}) async-start(), calls=%async_computation.3 | async-start | bytes 1114112 | tf_op jit(solution)/shard_map/all_gather | solution.py:102
  8.0 182.0 %all-gather.12.cloned.1.call-start = ((), (), s32[]{:S(2)}) async-start(), calls=%async_computation.4 | async-start | bytes 1114112 | tf_op jit(solution)/shard_map/all_gather | solution.py:103
  8.7 237.9 %all-gather.14.cloned.1.call-start = ((), (), s32[]{:S(2)}) async-start(), calls=%async_computation.5 | async-start | bytes 1114112 | tf_op jit(solution)/shard_map/all_gather | solution.py:104
  9.3 293.8 %all-gather.16.cloned.1.call-start = ((), (), s32[]{:S(2)}) async-start(), calls=%async_computation.6 | async-start | bytes 1114112 | tf_op jit(solution)/shard_map/all_gather | solution.py:105
  9.9 349.8 %all-gather.20.cloned.1.call-start = ((), (), s32[]{:S(2)}) async-start(), calls=%async_computation.8 | async-start | bytes 1114112 | tf_op jit(solution)/shard_map/all_gather | solution.py:154
  12.4 293.0 %all-to-all-start = ((bf16[16,64,512]{2,1,0:T(8,128)(2,1)}), bf16[16,64,512]{2,1,0:T(8,128)(2,1)S(1)}, u32[]{:S(2)}, u32[]{:S(2)}) async-start(bf16[16,64,512]{2,1,0:T(8,128)(2,1)} %stack.2), calls=%async_computation | async-start | bytes 2097152 | tf_op jit(solution)/shard_map/all_to_all | solution.py:107
  20.8 395.7 %all-gather.18.cloned.1.call-start = ((), (), s32[]{:S(2)}) async-start(), calls=%async_computation.7 | async-start | bytes 1114112 | tf_op jit(solution)/shard_map/all_gather | solution.py:153
  21.5 405.1 %reduce-scatter.2.cloned.1.call-start = ((), (), s32[]{:S(2)}) async-start(), calls=%async_computation.9 | async-start | bytes 1572864 | tf_op jit(solution)/shard_map/reduce_scatter | solution.py:40
  311.5 12.5 %collective-permute-start.2 = (bf16[1,512]{1,0:T(2,128)(2,1)S(1)}, bf16[1,512]{1,0:T(2,128)(2,1)S(1)}, u32[]{:S(2)}, u32[]{:S(2)}) collective-permute-start(bf16[1,512]{1,0:T(2,128)(2,1)S(1)} %get-tuple-element.13), channel_id=1, source_target_pairs={{0,2},{2,4},{4,6},{6,8},{8,10},{10,12},{12,14},{14,16},{16,18},{18... | collective-permute-start | bytes 3080 | tf_op jit(solution)/shard_map/ppermute | solution.py:32
  314.8 9.2 %collective-permute-start.3 = (bf16[1,512]{1,0:T(2,128)(2,1)S(1)}, bf16[1,512]{1,0:T(2,128)(2,1)S(1)}, u32[]{:S(2)}, u32[]{:S(2)}) collective-permute-start(bf16[1,512]{1,0:T(2,128)(2,1)S(1)} %get-tuple-element.14), channel_id=1, source_target_pairs={{2,0},{4,2},{6,4},{8,6},{10,8},{12,10},{14,12},{16,14},{18,16},{20... | collective-permute-start | bytes 3080 | tf_op jit(solution)/shard_map/ppermute | solution.py:33
  316.8 44.6 %collective-permute-start = (bf16[64,512]{1,0:T(8,128)(2,1)}, bf16[64,512]{1,0:T(8,128)(2,1)}, u32[]{:S(2)}, u32[]{:S(2)}) collective-permute-start(bf16[64,512]{1,0:T(8,128)(2,1)} %get-tuple-element.9), channel_id=1, source_target_pairs={{0,2},{2,4},{4,6},{6,8},{8,10},{10,12},{12,14},{14,16},{16,18},{18... | collective-permute-start | bytes 196616 | tf_op jit(solution)/shard_map/ppermute | solution.py:32
  322.0 39.5 %collective-permute-start.1 = (bf16[64,512]{1,0:T(8,128)(2,1)}, bf16[64,512]{1,0:T(8,128)(2,1)}, u32[]{:S(2)}, u32[]{:S(2)}) collective-permute-start(bf16[64,512]{1,0:T(8,128)(2,1)} %get-tuple-element.10), channel_id=1, source_target_pairs={{2,0},{4,2},{6,4},{8,6},{10,8},{12,10},{14,12},{16,14},{18,16},{20... | collective-permute-start | bytes 196616 | tf_op jit(solution)/shard_map/ppermute | solution.py:33
Sparse Core Ops, SparseCore 0:
  10.1 65.1 all-gather.7
  78.0 55.2 all-gather.9
  136.1 53.9 all-gather.11
  192.6 53.9 all-gather.13
  249.2 53.9 all-gather.15
  305.8 53.9 all-gather.19
  362.5 53.9 all-gather.17
  419.4 7.2 reduce-scatter.1
